TPU v7x, 128 devices: a whole 4x4x4 slice. The times are simulated.
128 devices in a mesh: sp: 32 (over z, y, core), tp: 4 (over x).
Axes of the slice: x: 4, y: 4, z: 4, core: 2. Of those that a mesh axis runs over, the one named last changes fastest.
Arguments:
- query_rows: bfloat16 [32768, 1024], P('sp', 'tp'), may hold values from -6 to 6
- key_rows: bfloat16 [32768, 1024], P('sp', 'tp'), may hold values from -6 to 6
- value_rows: bfloat16 [32768, 1024], P('sp', 'tp'), may hold values from -6 to 6
- input_gate: float32 [8, 32768], P('tp', 'sp'), may hold values from -4 to 255
- forget_gate: float32 [8, 32768], P('tp', 'sp'), may hold values from -3 to 20
- output_gate: bfloat16 [32768, 1024], P('sp', 'tp'), may hold values from -6 to 6
- documents: int32 [32768], P('sp'), may hold values from 0 to 7, never falling along the last dimension, each value on 1 to 6144 neighbouring positions
- residual: bfloat16 [32768, 2048], P(('sp', 'tp')), may hold values from -6 to 6
- out_weight: bfloat16 [1024, 2048], P('tp'), may hold values from -0.375 to 0.375
- norm_gain: bfloat16 [2048], replicated, may hold values from 0.099609375 to 1.8984375
- gate_weight: bfloat16 [2048, 5632], P('sp', 'tp'), may hold values from -0.125 to 0.125
- up_weight: bfloat16 [2048, 5632], P('sp', 'tp'), may hold values from -0.125 to 0.125
- down_weight: bfloat16 [5632, 2048], P('tp', 'sp'), may hold values from -0.15625 to 0.15625
Outputs:
- layer_out: bfloat16 [32768, 2048], P(('sp', 'tp'))
Inputs may be any that keep to these rules, and one draw needn't show every extreme that they name: `documents`: document numbers never fall along the positions; each document covers 1 to 6144 positions and one covers exactly 6144.
All inputs are finite; a program needn't handle non-finite values.
Results may differ from a plain program's by a relative error of at most 0.013.
Values may be sent and summed in bfloat16 or wider, within the bound.
A program may use at most 128 MiB of HBM per device.

v0:
```python
import jax
import jax.numpy as jnp
from jax import lax
from jax.sharding import Mesh
from jax.sharding import PartitionSpec as P

HD = 128
BLOCK = 128
SP = ("sp_0", "sp_1", "sp_2")
SP_TP = ("sp_0", "sp_1", "sp_2", "tp")
neg_large = -1e30
norm_eps = 1e-06
highest = lax.Precision.HIGHEST


def gather_turned(arrays, axis, dims):
    turned = [jnp.moveaxis(a, dim, 0) for a, dim in zip(arrays, dims)]
    both = jnp.concatenate([t.reshape(len(t), -1) for t in turned], axis=1)
    whole, at, finished = (lax.all_gather(both, axis, axis=0, tiled=True), 0, [])
    for t, dim in zip(turned, dims):
        slab = whole[:, at : at + t[0].size].reshape(-1, *t.shape[1:])
        finished.append(jnp.moveaxis(slab, 0, dim))
        at += t[0].size
    return tuple(finished)


def nothing_yet(array, identity):
    return jax.tree.map(
        lambda part, zero: jnp.zeros_like(part) + jnp.asarray(zero, part.dtype), array, identity
    )


def all_in_one(array, axis):
    leaves = jax.tree.leaves(array)
    sequence = sorted(range(len(leaves)), key=lambda k: -leaves[k].size)
    width = (1, *leaves[sequence[0]].shape)[-1]
    lines = [
        jnp.pad(leaves[k].reshape(-1), (0, -leaves[k].size % width)).reshape(-1, width)
        for k in sequence
    ]
    both, at, found = (lax.all_gather(jnp.concatenate(lines), axis), 0, {})
    for k, line in zip(sequence, lines):
        slab = both[:, at : at + len(line)].reshape(len(both), -1)
        found[k] = slab[:, : leaves[k].size].reshape(-1, *leaves[k].shape)
        at += len(line)
    numbers = iter(range(len(leaves)))
    return jax.tree.map(lambda _: found[next(numbers)], array)


def gathered_by_type(array, axis):
    leaves, found = (jax.tree.leaves(array), {})
    for leading, a in enumerate(leaves):
        if leading not in found:
            alike = [k for k, b in enumerate(leaves) if b.dtype == a.dtype]
            got = (
                all_in_one([leaves[k] for k in alike], axis)
                if len(alike) > 1
                else [lax.all_gather(a, axis)]
            )
            for k, b in zip(alike, got):
                found[k] = b
    numbers = iter(range(len(leaves)))
    return jax.tree.map(lambda _: found[next(numbers)], array)


def prefix_by_axis(array, axes, combine, identity):
    before = start = nothing_yet(array, identity)
    total = array
    for axis in reversed(axes):
        devices, position = (lax.axis_size(axis), lax.axis_index(axis))
        pieces = gathered_by_type(total, axis)
        inside, total = (start, start)
        for k in range(devices):
            passed = k < position
            total = combine(total, jax.tree.map(lambda part: part[k], pieces))
            inside = jax.tree.map(lambda new, old: jnp.where(passed, new, old), total, inside)
        before = combine(inside, before)
    return before


def block_step(carried, inputs):
    memory, normer, stab_prev, carry_doc = carried
    queries, key_float, value_float, gate_in, log_forget, docs = inputs
    cumlog = jnp.cumsum(log_forget, axis=1)
    length = docs.shape[0]
    target_positions = jnp.arange(length)
    same_doc = (docs[:, None] == docs[None, :]) & (
        target_positions[:, None] >= target_positions[None, :]
    )
    log_weight = jnp.where(
        same_doc[None], cumlog[:, :, None] - cumlog[:, None, :] + gate_in[:, None, :], neg_large
    )
    carried_log = jnp.where((docs == carry_doc)[None, :], cumlog + stab_prev[:, None], neg_large)
    stabilizer = jnp.maximum(carried_log, jnp.max(log_weight, axis=2))
    scores = jnp.einsum("lhd,shd->hls", queries, key_float, precision=highest)
    weighted = scores * jnp.exp(log_weight - stabilizer[:, :, None])
    carried_scale = jnp.exp(carried_log - stabilizer)
    numerator = carried_scale[:, :, None] * jnp.einsum(
        "lhd,hde->hle", queries, memory, precision=highest
    )
    numerator = numerator + jnp.einsum("hls,she->hle", weighted, value_float, precision=highest)
    denominator = carried_scale * jnp.einsum(
        "lhd,hd->hl", queries, normer, precision=highest
    ) + jnp.sum(weighted, axis=2)
    outputs = numerator / jnp.maximum(jnp.abs(denominator), 1.0)[:, :, None]
    last_doc = docs[-1]
    inject_log = jnp.where(
        (docs == last_doc)[None, :], cumlog[:, -1:] - cumlog + gate_in, neg_large
    )
    inject_max = jnp.max(inject_log, axis=1)
    weights = jnp.exp(inject_log - inject_max[:, None])
    continues = carry_doc == last_doc
    stab_new = jnp.where(continues, jnp.maximum(cumlog[:, -1] + stab_prev, inject_max), inject_max)
    decay_scale = jnp.where(continues, jnp.exp(cumlog[:, -1] + stab_prev - stab_new), 0.0)
    inject = jnp.exp(inject_max - stab_new)
    memory_step = jnp.einsum(
        "lhd,lhe->hde", key_float * weights.T[:, :, None], value_float, precision=highest
    )
    normer_step = jnp.einsum("hl,lhd->hd", weights, key_float, precision=highest)
    memory = decay_scale[:, None, None] * memory + inject[:, None, None] * memory_step
    normer = decay_scale[:, None] * normer + inject[:, None] * normer_step
    return ((memory, normer, stab_new, last_doc), jnp.transpose(outputs, (1, 0, 2)))


def run_blocks(queries, key_float, value_float, gate_in, log_forget, docs, start_state):
    length, heads, width = queries.shape
    count = length // BLOCK
    inputs = (
        queries.reshape(count, BLOCK, heads, width),
        key_float.reshape(count, BLOCK, heads, width),
        value_float.reshape(count, BLOCK, heads, width),
        jnp.moveaxis(gate_in.reshape(heads, count, BLOCK), 1, 0),
        jnp.moveaxis(log_forget.reshape(heads, count, BLOCK), 1, 0),
        docs.reshape(count, BLOCK),
    )
    final, outputs = lax.scan(block_step, start_state, inputs)
    return (outputs.reshape(length, heads, width), final)


def join_states(earlier, later_part):
    memory_early, normer_early, stab_early, total_early, doc_early = earlier
    memory_late, normer_late, stab_late, total_late, doc_late = later_part
    continues = doc_late == doc_early
    is_empty = doc_late < 0
    stab_both = jnp.where(continues, jnp.maximum(total_late + stab_early, stab_late), stab_late)
    scale_early = jnp.where(continues, jnp.exp(total_late + stab_early - stab_both), 0.0)
    scale_late = jnp.exp(stab_late - stab_both)
    memory = scale_early[:, None, None] * memory_early + scale_late[:, None, None] * memory_late
    normer = scale_early[:, None] * normer_early + scale_late[:, None] * normer_late
    return (
        jnp.where(is_empty, memory_early, memory),
        jnp.where(is_empty, normer_early, normer),
        jnp.where(is_empty, stab_early, stab_both),
        total_early + total_late,
        jnp.where(is_empty, doc_early, doc_late),
    )


def body(
    query_rows,
    key_rows,
    value_rows,
    input_gate,
    forget_gate,
    output_gate,
    documents,
    residual,
    out_weight,
    norm_gain,
    gate_weight,
    up_weight,
    down_weight,
):
    whole_gate, whole_up, whole_down = gather_turned(
        (gate_weight, up_weight, down_weight), SP, (0, 0, 1)
    )
    tokens = query_rows.shape[0]
    local_heads = input_gate.shape[0]
    queries = query_rows.astype(jnp.float32).reshape(tokens, local_heads, HD) * HD ** (-0.5)
    key_float = key_rows.astype(jnp.float32).reshape(tokens, local_heads, HD)
    value_float = value_rows.astype(jnp.float32).reshape(tokens, local_heads, HD)
    log_forget = jax.nn.log_sigmoid(forget_gate)
    cumlog = jnp.cumsum(log_forget, axis=1)
    total = cumlog[:, -1]
    last_doc = documents[-1]
    inject_log = jnp.where(
        (documents == last_doc)[None, :], total[:, None] - cumlog + input_gate, neg_large
    )
    inject_max = jnp.max(inject_log, axis=1)
    weights = jnp.exp(inject_log - inject_max[:, None])
    memory = jnp.einsum(
        "thd,the->hde", key_float * weights.T[:, :, None], value_float, precision=highest
    )
    normer = jnp.einsum("ht,thd->hd", weights, key_float, precision=highest)
    identity = (
        jnp.zeros_like(memory),
        jnp.zeros_like(normer),
        jnp.full_like(inject_max, neg_large),
        jnp.zeros_like(total),
        jnp.array(-1, jnp.int32),
    )
    before = prefix_by_axis(
        (memory, normer, inject_max, total, last_doc), SP, join_states, identity
    )
    cells, final = run_blocks(
        queries,
        key_float,
        value_float,
        input_gate,
        log_forget,
        documents,
        (before[0], before[1], before[2], before[4]),
    )
    gated = (cells.reshape(tokens, -1) * jax.nn.sigmoid(output_gate.astype(jnp.float32))).astype(
        jnp.bfloat16
    )
    mine = lax.all_to_all(gated, "tp", split_axis=0, concat_axis=1, tiled=True)
    projected = jnp.dot(
        mine,
        lax.all_gather(out_weight, "tp", axis=0, tiled=True),
        preferred_element_type=jnp.float32,
    )
    stream = residual.astype(jnp.float32) + projected
    normed = stream * lax.rsqrt(jnp.mean(stream * stream, axis=1, keepdims=True) + norm_eps)
    normed = (normed * norm_gain.astype(jnp.float32)).astype(jnp.bfloat16)
    rows_all = lax.all_gather(normed, "tp", axis=0, tiled=True)
    gate_act = jnp.dot(rows_all, whole_gate, preferred_element_type=jnp.float32)
    up_act = jnp.dot(rows_all, whole_up, preferred_element_type=jnp.float32)
    hidden = (jax.nn.silu(gate_act) * up_act).astype(jnp.bfloat16)
    partial_sum = jnp.dot(hidden, whole_down, preferred_element_type=jnp.float32)
    down = lax.psum_scatter(
        partial_sum.astype(jnp.bfloat16), "tp", scatter_dimension=0, tiled=True
    ).astype(jnp.float32)
    return (stream + 0.5 * down).astype(jnp.bfloat16)


def solution(mesh):
    torus = Mesh(mesh.devices.reshape(4, 4, 2, mesh.shape["tp"]), ("sp_0", "sp_1", "sp_2", "tp"))
    in_specs = (
        P(SP, "tp"),
        P(SP, "tp"),
        P(SP, "tp"),
        P("tp", SP),
        P("tp", SP),
        P(SP, "tp"),
        P(SP),
        P(SP_TP, None),
        P("tp", None),
        P(),
        P(SP, "tp"),
        P(SP, "tp"),
        P("tp", SP),
    )
    out_specs = P(SP_TP, None)
    return jax.shard_map(body, mesh=torus, in_specs=in_specs, out_specs=out_specs, check_vma=False)
```

profile of v0, /device:TPU:1, one launch (start us, length us, event | category | flops | bytes accessed | tf_op | source)
XLA Modules:
  0.0 448.9 jit_solution(14347902271754953552)
XLA Ops:
  8.7 1.2 dynamic-slice
  10.0 1.9 slice_dynamic-update-slice_fusion
  11.9 1.3 broadcast_compare_fusion
  15.4 1.2 copy.56
  16.7 1.4 fusion.34
  18.0 1.7 fusion.32
  19.8 3.2 all-gather.3
  23.6 1.8 all-reduce.6
  31.0 11.8 %all-gather.4 = f32[4,260,128]{2,1,0:T(8,128)S(1)} all-gather(f32[1,260,128]{2,1,0:T(8,128)S(1)} %maximum_bitcast_fusion.1), channel_id=3, replica_groups=mesh['sp_0'=4,'sp_1'=4,'sp_2'=2,'tp'=4] {'sp_1'}, dimensions={0}, use_global_device_ids=true | all-gather | bytes 665600 | tf_op jit(solution)/shard_map/all_gather | solution.py:41
  45.5 6.5 %all-reduce.7 = s32[4]{0:T(128)S(1)} all-reduce(s32[4]{0:T(128)S(1)} %dynamic-update-slice.1), channel_id=1, replica_groups=mesh['sp_0'=4,'sp_1'=4,'sp_2'=2,'tp'=4] {'sp_1'}, use_global_device_ids=true, to_apply=%add.7 | all-reduce | flops 4 | bytes 32
  61.6 11.7 %all-gather.5 = f32[4,260,128]{2,1,0:T(8,128)S(1)} all-gather(f32[1,260,128]{2,1,0:T(8,128)S(1)} %maximum_bitcast_fusion.2), channel_id=4, replica_groups=mesh['sp_0'=4,'sp_1'=4,'sp_2'=2,'tp'=4] {'sp_0'}, dimensions={0}, use_global_device_ids=true | all-gather | bytes 665600 | tf_op jit(solution)/shard_map/all_gather | solution.py:41
  74.2 1.5 reshape.2044
  75.6 1.2 dynamic-slice.2
  77.6 7.2 %all-reduce.8 = s32[4]{0:T(128)S(1)} all-reduce(s32[4]{0:T(128)S(1)} %dynamic-update-slice.2), channel_id=1, replica_groups=mesh['sp_0'=4,'sp_1'=4,'sp_2'=2,'tp'=4] {'sp_0'}, use_global_device_ids=true, to_apply=%add.8 | all-reduce | flops 4 | bytes 32
  92.9 1.1 convert_multiply_fusion
  94.1 1.5 reshape.2046
  95.9 1.8 add_select_fusion.3
  97.7 112.4 %while.18 = (s32[]{:T(128)}, f32[2,128,128]{2,1,0:T(8,128)S(1)}, f32[2,128]{1,0:T(2,128)S(1)}, f32[2]{0:T(128)S(1)}, s32[]{:T(128)}, /*index=5*/f32[8,128,2,128]...) while((s32[]{:T(128)}, f32[2,128,128]{2,1,0:T(8,128)S(1)}, ...), condition=%wide.region_8.9_spmd, body=%wide.region_3.8_spmd.sunk | while | flops 202756624 | bytes 3499011 | solution.py:136
  102.2 0.9 constant_dynamic-slice_fusion.10
  103.3 0.9 constant_dynamic-slice_fusion.9
  106.4 4.7 %dynamic_update_slice.5 = f32[8,128,2,128]{1,0,3,2:T(8,128)} dynamic-update-slice(f32[8,128,2,128]{1,0,3,2:T(8,128)} %get-tuple-element.360, f32[1,128,2,128]{1,0,3,2:T(1,128)S(1)} %copy.134, s32[]{:T(128)S(6)} %copy.145, s32[]{:T(128)} %constant.31.clone.1..sunk, s32[]{:T(128)} %constant.31.clone.1..sunk, s32[]{:T(128)} %constant.31.clone.1..sunk) | dynamic-update-slice | bytes 262148 | tf_op jit(solution)/shard_map/while/body/jit(dynamic_update_index_in_dim)/dynamic_update_slice | solution.py:136
  116.2 0.9 constant_dynamic-slice_fusion.10
  117.3 0.9 constant_dynamic-slice_fusion.9
  120.5 4.7 %dynamic_update_slice.5 = f32[8,128,2,128]{1,0,3,2:T(8,128)} dynamic-update-slice(f32[8,128,2,128]{1,0,3,2:T(8,128)} %get-tuple-element.360, f32[1,128,2,128]{1,0,3,2:T(1,128)S(1)} %copy.134, s32[]{:T(128)S(6)} %copy.145, s32[]{:T(128)} %constant.31.clone.1..sunk, s32[]{:T(128)} %constant.31.clone.1..sunk, s32[]{:T(128)} %constant.31.clone.1..sunk) | dynamic-update-slice | bytes 262148 | tf_op jit(solution)/shard_map/while/body/jit(dynamic_update_index_in_dim)/dynamic_update_slice | solution.py:136
  130.2 0.9 constant_dynamic-slice_fusion.10
  131.4 0.9 constant_dynamic-slice_fusion.9
  134.5 4.7 %dynamic_update_slice.5 = f32[8,128,2,128]{1,0,3,2:T(8,128)} dynamic-update-slice(f32[8,128,2,128]{1,0,3,2:T(8,128)} %get-tuple-element.360, f32[1,128,2,128]{1,0,3,2:T(1,128)S(1)} %copy.134, s32[]{:T(128)S(6)} %copy.145, s32[]{:T(128)} %constant.31.clone.1..sunk, s32[]{:T(128)} %constant.31.clone.1..sunk, s32[]{:T(128)} %constant.31.clone.1..sunk) | dynamic-update-slice | bytes 262148 | tf_op jit(solution)/shard_map/while/body/jit(dynamic_update_index_in_dim)/dynamic_update_slice | solution.py:136
  145.4 0.9 constant_dynamic-slice_fusion.9
  148.6 4.7 %dynamic_update_slice.5 = f32[8,128,2,128]{1,0,3,2:T(8,128)} dynamic-update-slice(f32[8,128,2,128]{1,0,3,2:T(8,128)} %get-tuple-element.360, f32[1,128,2,128]{1,0,3,2:T(1,128)S(1)} %copy.134, s32[]{:T(128)S(6)} %copy.145, s32[]{:T(128)} %constant.31.clone.1..sunk, s32[]{:T(128)} %constant.31.clone.1..sunk, s32[]{:T(128)} %constant.31.clone.1..sunk) | dynamic-update-slice | bytes 262148 | tf_op jit(solution)/shard_map/while/body/jit(dynamic_update_index_in_dim)/dynamic_update_slice | solution.py:136
  159.5 0.9 constant_dynamic-slice_fusion.9
  162.6 4.7 %dynamic_update_slice.5 = f32[8,128,2,128]{1,0,3,2:T(8,128)} dynamic-update-slice(f32[8,128,2,128]{1,0,3,2:T(8,128)} %get-tuple-element.360, f32[1,128,2,128]{1,0,3,2:T(1,128)S(1)} %copy.134, s32[]{:T(128)S(6)} %copy.145, s32[]{:T(128)} %constant.31.clone.1..sunk, s32[]{:T(128)} %constant.31.clone.1..sunk, s32[]{:T(128)} %constant.31.clone.1..sunk) | dynamic-update-slice | bytes 262148 | tf_op jit(solution)/shard_map/while/body/jit(dynamic_update_index_in_dim)/dynamic_update_slice | solution.py:136
  173.5 0.9 constant_dynamic-slice_fusion.9
  176.6 4.7 %dynamic_update_slice.5 = f32[8,128,2,128]{1,0,3,2:T(8,128)} dynamic-update-slice(f32[8,128,2,128]{1,0,3,2:T(8,128)} %get-tuple-element.360, f32[1,128,2,128]{1,0,3,2:T(1,128)S(1)} %copy.134, s32[]{:T(128)S(6)} %copy.145, s32[]{:T(128)} %constant.31.clone.1..sunk, s32[]{:T(128)} %constant.31.clone.1..sunk, s32[]{:T(128)} %constant.31.clone.1..sunk) | dynamic-update-slice | bytes 262148 | tf_op jit(solution)/shard_map/while/body/jit(dynamic_update_index_in_dim)/dynamic_update_slice | solution.py:136
  187.6 0.9 constant_dynamic-slice_fusion.9
  190.7 4.7 %dynamic_update_slice.5 = f32[8,128,2,128]{1,0,3,2:T(8,128)} dynamic-update-slice(f32[8,128,2,128]{1,0,3,2:T(8,128)} %get-tuple-element.360, f32[1,128,2,128]{1,0,3,2:T(1,128)S(1)} %copy.134, s32[]{:T(128)S(6)} %copy.145, s32[]{:T(128)} %constant.31.clone.1..sunk, s32[]{:T(128)} %constant.31.clone.1..sunk, s32[]{:T(128)} %constant.31.clone.1..sunk) | dynamic-update-slice | bytes 262148 | tf_op jit(solution)/shard_map/while/body/jit(dynamic_update_index_in_dim)/dynamic_update_slice | solution.py:136
  201.6 0.9 constant_dynamic-slice_fusion.9
  204.7 4.7 %dynamic_update_slice.5 = f32[8,128,2,128]{1,0,3,2:T(8,128)} dynamic-update-slice(f32[8,128,2,128]{1,0,3,2:T(8,128)} %get-tuple-element.360, f32[1,128,2,128]{1,0,3,2:T(1,128)S(1)} %copy.134, s32[]{:T(128)S(6)} %copy.145, s32[]{:T(128)} %constant.31.clone.1..sunk, s32[]{:T(128)} %constant.31.clone.1..sunk, s32[]{:T(128)} %constant.31.clone.1..sunk) | dynamic-update-slice | bytes 262148 | tf_op jit(solution)/shard_map/while/body/jit(dynamic_update_index_in_dim)/dynamic_update_slice | solution.py:136
  210.4 1.6 fusion.31
  212.8 3.7 all-to-all-start
  216.5 6.9 %all-to-all-done = bf16[4,256,256]{1,2,0:T(8,128)(2,1)S(1)} async-done(((bf16[4,256,256]{1,2,0:T(8,128)(2,1)}), bf16[4,256,256]{1,2,0:T(8,128)(2,1)S(1)}, u32[]{:S(2)}, u32[]{:S(2)}) %all-to-all-start) | async-done | bytes 524320 | tf_op jit(solution)/shard_map/all_to_all | solution.py:217
  223.4 3.9 multiply_reduce_fusion
  227.4 1.2 multiply_convert_fusion.1
  229.8 52.7 %all-gather.12.cloned.1.call-done = bf16[1024,2048]{1,0:T(8,128)(2,1)} async-done(((bf16[256,2048]{1,0:T(8,128)(2,1)}), bf16[1024,2048]{1,0:T(8,128)(2,1)}) %all-gather.12.cloned.1.call-update) | async-done | bytes 4194320 | tf_op jit(solution)/shard_map/all_gather | solution.py:226
  282.5 77.2 %all-gather.14.cloned.1.call-done = bf16[2048,4224]{1,0:T(8,128)(2,1)} async-done(((bf16[64,4224]{1,0:T(8,128)(2,1)}), bf16[2048,4224]{1,0:T(8,128)(2,1)}) %all-gather.14.cloned.1.call-update) | async-done | bytes 17301520 | tf_op jit(solution)/shard_map/all_gather | solution.py:19
  359.6 11.7 %fusion.21 = f32[1024,1408]{1,0:T(8,128)} fusion(bf16[1024,2048]{1,0:T(8,128)(2,1)} %all-gather.12.cloned.1.call-done, bf16[2048,4224]{1,0:T(8,128)(2,1)} %all-gather.14.cloned.1.call-done), kind=kOutput, calls=%fused_computation.48 | convolution fusion | flops 5905580032 | bytes 15728640 | tf_op jit(solution)/shard_map/dot_general | solution.py:227
  371.3 22.7 %fusion.25 = bf16[1024,2048]{1,0:T(8,128)(2,1)} fusion(bf16[2048,4224]{1,0:T(8,128)(2,1)} %all-gather.14.cloned.1.call-done, f32[1024,1408]{1,0:T(8,128)} %fusion.21, bf16[1024,2048]{1,0:T(8,128)(2,1)} %all-gather.12.cloned.1.call-done), kind=kOutput, calls=%fused_computation.51 | convolution fusion | flops 11821907968 | bytes 25690112 | tf_op jit(solution)/shard_map/dot_general | solution.py:230
  394.0 45.9 %reduce-scatter.2.cloned.1.call-done = bf16[256,2048]{1,0:T(8,128)(2,1)} async-done(((bf16[1024,2048]{1,0:T(8,128)(2,1)}), bf16[256,2048]{1,0:T(8,128)(2,1)}) %reduce-scatter.2.cloned.1.call-update) | async-done | bytes 1048592 | tf_op jit(solution)/shard_map/reduce_scatter | solution.py:231
  439.9 2.5 add_convert_fusion
  (279 shorter events, 69.0 us)
Async XLA Ops:
  6.5 37.1 %copy-start.9 = (u32[128]{0:T(128)S(1)}, u32[128]{0:T(128)}, u32[]{:S(2)}) copy-start(u32[128]{0:T(128)} %constant.104) | copy-start | bytes 1540
  6.5 38.5 %copy-start.1 = (bf16[1024,256]{1,0:T(8,128)(2,1)S(1)}, bf16[1024,256]{1,0:T(8,128)(2,1)}, u32[]{:S(2)}) copy-start(bf16[1024,256]{1,0:T(8,128)(2,1)} %param.17) | copy-start | bytes 1572868
  6.5 216.9 %all-gather.10.cloned.1.call-start = ((), (), s32[]{:S(2)}) async-start(), calls=%async_computation.2 | async-start | bytes 5242880 | tf_op jit(solution)/shard_map/all_gather | solution.py:220
  19.7 54.4 %copy-start = (bf16[1024,256]{1,0:T(8,128)(2,1)S(1)}, bf16[1024,256]{1,0:T(8,128)(2,1)}, u32[]{:S(2)}) copy-start(bf16[1024,256]{1,0:T(8,128)(2,1)} %param.16) | copy-start | bytes 1572868
  30.2 0.5 copy-start.7
  60.6 0.6 copy-start.8
  97.7 112.4 %copy-start.2 = (bf16[1024,256]{1,0:T(8,128)(2,1)S(1)}, bf16[1024,256]{1,0:T(8,128)(2,1)}, u32[]{:S(2)}) copy-start(bf16[1024,256]{1,0:T(8,128)(2,1)} %param.20) | copy-start | bytes 1572868
  210.1 6.4 %copy-start.6 = (bf16[2048]{0:T(1024)(128)(2,1)S(1)}, bf16[2048]{0:T(1024)(128)(2,1)}, u32[]{:S(2)}) copy-start(bf16[2048]{0:T(1024)(128)(2,1)} %param.24) | copy-start | bytes 12292
  212.8 10.7 %all-to-all-start = ((bf16[4,256,256]{1,2,0:T(8,128)(2,1)}), bf16[4,256,256]{1,2,0:T(8,128)(2,1)S(1)}, u32[]{:S(2)}, u32[]{:S(2)}) async-start(bf16[4,256,256]{1,2,0:T(8,128)(2,1)} %bitcast.516), calls=%async_computation | async-start | bytes 1048576 | tf_op jit(solution)/shard_map/all_to_all | solution.py:217
  216.5 66.0 %all-gather.12.cloned.1.call-start = ((), (), s32[]{:S(2)}) async-start(), calls=%async_computation.3 | async-start | bytes 5242880 | tf_op jit(solution)/shard_map/all_gather | solution.py:226
  227.3 1.3 copy-start.3
  227.3 1.3 copy-start.4
  227.3 1.3 copy-start.5
  228.6 131.1 %all-gather.14.cloned.1.call-start = ((), (), s32[]{:S(2)}) async-start(), calls=%async_computation.4 | async-start | bytes 17842176 | tf_op jit(solution)/shard_map/all_gather | solution.py:19
  229.5 210.4 %reduce-scatter.2.cloned.1.call-start = ((), (), s32[]{:S(2)}) async-start(), calls=%async_computation.5 | async-start | bytes 5242880 | tf_op jit(solution)/shard_map/reduce_scatter | solution.py:231
Sparse Core Ops, SparseCore 0:
  9.0 51.1 all-gather.9
  228.7 53.7 all-gather.11
  284.7 74.8 all-gather.13
  394.2 45.7 reduce-scatter.1
where the time goes:
time: 451 us; the launch traced here: 449 us
  waiting for transfers between devices  183 us (41%)
  local copies, waits for them, and re-layouts  78.3 us (17%)
  matrix products  58.1 us (13%)
  blocking collectives  42.2 us (9%)
  other arithmetic  39.2 us (9%)
  between operations  32.8 us (7%)
  loops' own time  10.8 us (2%)
    all_gather x1, waiting for transfers between devices, gather_turned(): lax.all_gather(both, axis, axis=0, tiled=True)  77.2 us
    all_gather x1, waiting for transfers between devices, body(): rows_all = lax.all_gather(normed, 'tp', axis=0, tiled=True)  52.7 us
    reduce_scatter x1, waiting for transfers between devices, body(): lax.psum_scatter(partial_sum.astype(jnp.bfloat16), 'tp', scatter_dimensio...  45.9 us
    dynamic_update_slice x16, local copies, waits for them, and re-layouts, run_blocks(): final, outputs = lax.scan(block_step, start_state, inputs)  38.7 us
    all_gather x3, blocking collectives, all_in_one(): both, at, found = (lax.all_gather(jnp.concatenate(lines), axis), 0, {})  26.6 us
    dot_general x1, matrix products, body(): jnp.dot(hidden, whole_down, preferred_element_type=jnp.float32)  22.7 us
    unnamed x3, blocking collectives  15.6 us
    dynamic_slice x16, local copies, waits for them, and re-layouts, run_blocks(): final, outputs = lax.scan(block_step, start_state, inputs)  14.8 us
  transfers between devices with their start and end apart: 5, of which 4 were waited for; matrix products, arithmetic and copies ran while one was open for 30% of the time, Pallas kernels for 0%

commit v1 on v0

--- a/solution.py
+++ b/solution.py
@@ -11,6 +11,17 @@
 neg_large = -1e30
 norm_eps = 1e-06
 highest = lax.Precision.HIGHEST
+
+
+def pass_along(x, name, d):
+    size = lax.axis_size(name)
+    right = [(i, (i + 1) % size) for i in range(size)]
+    blocks = [x]
+    for far in range(1, size):
+        blocks = [lax.ppermute(blocks[0], name, right), *blocks]
+    out = jnp.concatenate(blocks, axis=d)
+    shift = (lax.axis_index(name) + 1) * blocks[-1].shape[d]
+    return jnp.roll(out, shift, axis=d)
 
 
 def gather_turned(arrays, axis, dims):
@@ -223,7 +234,7 @@
     stream = residual.astype(jnp.float32) + projected
     normed = stream * lax.rsqrt(jnp.mean(stream * stream, axis=1, keepdims=True) + norm_eps)
     normed = (normed * norm_gain.astype(jnp.float32)).astype(jnp.bfloat16)
-    rows_all = lax.all_gather(normed, "tp", axis=0, tiled=True)
+    rows_all = pass_along(normed, "tp", 0)
     gate_act = jnp.dot(rows_all, whole_gate, preferred_element_type=jnp.float32)
     up_act = jnp.dot(rows_all, whole_up, preferred_element_type=jnp.float32)
     hidden = (jax.nn.silu(gate_act) * up_act).astype(jnp.bfloat16)

time: 451 us -> 396 us (0.88)
  waiting for transfers between devices: 183 us -> 123 us
  local copies, waits for them, and re-layouts: 78.3 us -> 83.6 us
    all_gather x1, waiting for transfers between devices: 77.2 us -> 0.01 us  [gather_turned(): lax.all_gather(both, axis, axis=0, tiled=True)]
    ppermute x0 -> x3, waiting for transfers between devices: none -> 60.5 us  [pass_along(): blocks = [lax.ppermute(blocks[0], name, right), *blocks]]
    all_gather x1 -> x0, waiting for transfers between devices: 52.7 us -> none  [body(): rows_all = lax.all_gather(normed, 'tp', axis=0, tiled=True)]
    unnamed x31 -> x35, local copies, waits for them, and re-layouts: 7.75 us -> 20.2 us
    reduce_scatter x1, waiting for transfers between devices: 45.9 us -> 54.6 us  [body(): lax.psum_scatter(partial_sum.astype(jnp.bfloat16), 'tp', scatter_dimensio...]
    dynamic_slice x16, local copies, waits for them, and re-layouts: 14.8 us -> 8.17 us  [run_blocks(): final, outputs = lax.scan(block_step, start_state, inputs)]
  transfers between devices with their start and end apart: 5 -> 7, of which waited for: 4 -> 5; matrix products, arithmetic and copies ran while one was open for 30% -> 37% of each run, Pallas kernels for 0% -> 0%
where the time goes in v1:
time: 396 us; the launch traced here: 393 us
  waiting for transfers between devices  123 us (31%)
  local copies, waits for them, and re-layouts  83.6 us (21%)
  matrix products  56.2 us (14%)
  blocking collectives  43.8 us (11%)
  other arithmetic  41 us (10%)
  between operations  32.1 us (8%)
  loops' own time  9.67 us (2%)
  starting transfers between devices  4.11 us (1%)
    ppermute x3, waiting for transfers between devices, pass_along(): blocks = [lax.ppermute(blocks[0], name, right), *blocks]  60.5 us
    reduce_scatter x1, waiting for transfers between devices, body(): lax.psum_scatter(partial_sum.astype(jnp.bfloat16), 'tp', scatter_dimensio...  54.6 us
    dynamic_update_slice x16, local copies, waits for them, and re-layouts, run_blocks(): final, outputs = lax.scan(block_step, start_state, inputs)  38.9 us
    all_gather x3, blocking collectives, all_in_one(): both, at, found = (lax.all_gather(jnp.concatenate(lines), axis), 0, {})  26 us
    dot_general x1, matrix products, body(): jnp.dot(hidden, whole_down, preferred_element_type=jnp.float32)  20.6 us
    unnamed x35, local copies, waits for them, and re-layouts  20.2 us
    unnamed x3, blocking collectives  17.9 us
    dot_general x1, matrix products, body(): gate_act = jnp.dot(rows_all, whole_gate, preferred_element_type=jnp.float32)  11.7 us
  transfers between devices with their start and end apart: 7, of which 5 were waited for; matrix products, arithmetic and copies ran while one was open for 37% of the time, Pallas kernels for 0%

profile of v1, /device:TPU:1, one launch (start us, length us, event | category | flops | bytes accessed | tf_op | source)
XLA Modules:
  0.0 393.3 jit_solution(17342517165000882984)
XLA Ops:
  7.3 1.9 pad_maximum_fusion
  9.3 1.3 dynamic-slice
  10.6 1.9 slice_dynamic-update-slice_fusion
  12.5 2.9 all-reduce.6
  17.9 1.2 dynamic-slice.1
  21.6 7.2 %all-reduce.7 = s32[4]{0:T(128)S(1)} all-reduce(s32[4]{0:T(128)S(1)} %dynamic-update-slice.1), channel_id=1, replica_groups=mesh['sp_0'=4,'sp_1'=4,'sp_2'=2,'tp'=4] {'sp_1'}, use_global_device_ids=true, to_apply=%add.7 | all-reduce | flops 4 | bytes 32
  36.8 1.3 broadcast_compare_fusion
  41.0 1.3 copy.56
  42.3 1.4 fusion.40
  43.7 1.7 fusion.38
  45.5 3.9 all-gather.3
  49.8 10.8 %all-gather.4 = f32[4,260,128]{2,1,0:T(8,128)S(1)} all-gather(f32[1,260,128]{2,1,0:T(8,128)S(1)} %maximum_bitcast_fusion.1), channel_id=3, replica_groups=mesh['sp_0'=4,'sp_1'=4,'sp_2'=2,'tp'=4] {'sp_1'}, dimensions={0}, use_global_device_ids=true | all-gather | bytes 665600 | tf_op jit(solution)/shard_map/all_gather | solution.py:52
  61.1 11.3 %all-gather.5 = f32[4,260,128]{2,1,0:T(8,128)S(1)} all-gather(f32[1,260,128]{2,1,0:T(8,128)S(1)} %maximum_bitcast_fusion.2), channel_id=4, replica_groups=mesh['sp_0'=4,'sp_1'=4,'sp_2'=2,'tp'=4] {'sp_0'}, dimensions={0}, use_global_device_ids=true | all-gather | bytes 665600 | tf_op jit(solution)/shard_map/all_gather | solution.py:52
  76.2 1.5 reshape.2045
  79.1 7.8 %all-reduce.8 = s32[4]{0:T(128)S(1)} all-reduce(s32[4]{0:T(128)S(1)} %dynamic-update-slice.2), channel_id=1, replica_groups=mesh['sp_0'=4,'sp_1'=4,'sp_2'=2,'tp'=4] {'sp_0'}, use_global_device_ids=true, to_apply=%add.8 | all-reduce | flops 4 | bytes 32
  95.1 1.1 convert_multiply_fusion
  96.3 1.5 reshape.2046
  97.7 1.4 copy.45
  100.2 1.7 add_select_fusion.3
  101.9 103.5 %while.18 = (s32[]{:T(128)}, f32[2,128,128]{2,1,0:T(8,128)S(1)}, f32[2,128]{1,0:T(2,128)S(1)}, f32[2]{0:T(128)S(1)}, s32[]{:T(128)}, /*index=5*/f32[8,128,2,128]...) while((s32[]{:T(128)}, f32[2,128,128]{2,1,0:T(8,128)S(1)}, ...), condition=%wide.region_8.9_spmd, body=%wide.region_3.8_spmd.sunk | while | flops 202756624 | bytes 3499003 | solution.py:147
  108.9 4.8 %dynamic_update_slice.5 = f32[8,128,2,128]{1,0,3,2:T(8,128)} dynamic-update-slice(f32[8,128,2,128]{1,0,3,2:T(8,128)} %get-tuple-element.360, f32[1,128,2,128]{1,0,3,2:T(1,128)S(1)} %copy.134, s32[]{:T(128)} %get-tuple-element.355, s32[]{:T(128)} %constant.61.clone.1..sunk, s32[]{:T(128)} %constant.61.clone.1..sunk, s32[]{:T(128)} %constant.61.clone.1..sunk) | dynamic-update-slice | bytes 262148 | tf_op jit(solution)/shard_map/while/body/jit(dynamic_update_index_in_dim)/dynamic_update_slice | solution.py:147
  121.9 4.8 %dynamic_update_slice.5 = f32[8,128,2,128]{1,0,3,2:T(8,128)} dynamic-update-slice(f32[8,128,2,128]{1,0,3,2:T(8,128)} %get-tuple-element.360, f32[1,128,2,128]{1,0,3,2:T(1,128)S(1)} %copy.134, s32[]{:T(128)} %get-tuple-element.355, s32[]{:T(128)} %constant.61.clone.1..sunk, s32[]{:T(128)} %constant.61.clone.1..sunk, s32[]{:T(128)} %constant.61.clone.1..sunk) | dynamic-update-slice | bytes 262148 | tf_op jit(solution)/shard_map/while/body/jit(dynamic_update_index_in_dim)/dynamic_update_slice | solution.py:147
  132.2 1.1 constant_dynamic-slice_fusion.9
  134.9 4.8 %dynamic_update_slice.5 = f32[8,128,2,128]{1,0,3,2:T(8,128)} dynamic-update-slice(f32[8,128,2,128]{1,0,3,2:T(8,128)} %get-tuple-element.360, f32[1,128,2,128]{1,0,3,2:T(1,128)S(1)} %copy.134, s32[]{:T(128)} %get-tuple-element.355, s32[]{:T(128)} %constant.61.clone.1..sunk, s32[]{:T(128)} %constant.61.clone.1..sunk, s32[]{:T(128)} %constant.61.clone.1..sunk) | dynamic-update-slice | bytes 262148 | tf_op jit(solution)/shard_map/while/body/jit(dynamic_update_index_in_dim)/dynamic_update_slice | solution.py:147
  147.9 4.7 %dynamic_update_slice.5 = f32[8,128,2,128]{1,0,3,2:T(8,128)} dynamic-update-slice(f32[8,128,2,128]{1,0,3,2:T(8,128)} %get-tuple-element.360, f32[1,128,2,128]{1,0,3,2:T(1,128)S(1)} %copy.134, s32[]{:T(128)} %get-tuple-element.355, s32[]{:T(128)} %constant.61.clone.1..sunk, s32[]{:T(128)} %constant.61.clone.1..sunk, s32[]{:T(128)} %constant.61.clone.1..sunk) | dynamic-update-slice | bytes 262148 | tf_op jit(solution)/shard_map/while/body/jit(dynamic_update_index_in_dim)/dynamic_update_slice | solution.py:147
  160.8 4.7 %dynamic_update_slice.5 = f32[8,128,2,128]{1,0,3,2:T(8,128)} dynamic-update-slice(f32[8,128,2,128]{1,0,3,2:T(8,128)} %get-tuple-element.360, f32[1,128,2,128]{1,0,3,2:T(1,128)S(1)} %copy.134, s32[]{:T(128)} %get-tuple-element.355, s32[]{:T(128)} %constant.61.clone.1..sunk, s32[]{:T(128)} %constant.61.clone.1..sunk, s32[]{:T(128)} %constant.61.clone.1..sunk) | dynamic-update-slice | bytes 262148 | tf_op jit(solution)/shard_map/while/body/jit(dynamic_update_index_in_dim)/dynamic_update_slice | solution.py:147
  173.7 4.7 %dynamic_update_slice.5 = f32[8,128,2,128]{1,0,3,2:T(8,128)} dynamic-update-slice(f32[8,128,2,128]{1,0,3,2:T(8,128)} %get-tuple-element.360, f32[1,128,2,128]{1,0,3,2:T(1,128)S(1)} %copy.134, s32[]{:T(128)} %get-tuple-element.355, s32[]{:T(128)} %constant.61.clone.1..sunk, s32[]{:T(128)} %constant.61.clone.1..sunk, s32[]{:T(128)} %constant.61.clone.1..sunk) | dynamic-update-slice | bytes 262148 | tf_op jit(solution)/shard_map/while/body/jit(dynamic_update_index_in_dim)/dynamic_update_slice | solution.py:147
  186.6 4.7 %dynamic_update_slice.5 = f32[8,128,2,128]{1,0,3,2:T(8,128)} dynamic-update-slice(f32[8,128,2,128]{1,0,3,2:T(8,128)} %get-tuple-element.360, f32[1,128,2,128]{1,0,3,2:T(1,128)S(1)} %copy.134, s32[]{:T(128)} %get-tuple-element.355, s32[]{:T(128)} %constant.61.clone.1..sunk, s32[]{:T(128)} %constant.61.clone.1..sunk, s32[]{:T(128)} %constant.61.clone.1..sunk) | dynamic-update-slice | bytes 262148 | tf_op jit(solution)/shard_map/while/body/jit(dynamic_update_index_in_dim)/dynamic_update_slice | solution.py:147
  199.5 4.7 %dynamic_update_slice.5 = f32[8,128,2,128]{1,0,3,2:T(8,128)} dynamic-update-slice(f32[8,128,2,128]{1,0,3,2:T(8,128)} %get-tuple-element.360, f32[1,128,2,128]{1,0,3,2:T(1,128)S(1)} %copy.134, s32[]{:T(128)} %get-tuple-element.355, s32[]{:T(128)} %constant.61.clone.1..sunk, s32[]{:T(128)} %constant.61.clone.1..sunk, s32[]{:T(128)} %constant.61.clone.1..sunk) | dynamic-update-slice | bytes 262148 | tf_op jit(solution)/shard_map/while/body/jit(dynamic_update_index_in_dim)/dynamic_update_slice | solution.py:147
  205.4 1.6 fusion.37
  207.8 3.7 all-to-all-start
  211.6 6.9 %all-to-all-done = bf16[4,256,256]{1,2,0:T(8,128)(2,1)S(1)} async-done(((bf16[4,256,256]{1,2,0:T(8,128)(2,1)}), bf16[4,256,256]{1,2,0:T(8,128)(2,1)S(1)}, u32[]{:S(2)}, u32[]{:S(2)}) %all-to-all-start) | async-done | bytes 524320 | tf_op jit(solution)/shard_map/all_to_all | solution.py:228
  218.5 3.9 multiply_reduce_fusion
  223.0 17.1 %collective-permute-done = bf16[256,2048]{1,0:T(8,128)(2,1)S(1)} collective-permute-done((bf16[256,2048]{1,0:T(8,128)(2,1)S(1)}, bf16[256,2048]{1,0:T(8,128)(2,1)S(1)}, u32[]{:S(2)}, u32[]{:S(2)}) %collective-permute-start) | collective-permute-done | bytes 1048608 | tf_op jit(solution)/shard_map/ppermute | solution.py:21
  240.1 21.7 %collective-permute-done.1 = bf16[256,2048]{1,0:T(8,128)(2,1)} collective-permute-done((bf16[256,2048]{1,0:T(8,128)(2,1)S(1)}, bf16[256,2048]{1,0:T(8,128)(2,1)}, u32[]{:S(2)}, u32[]{:S(2)}) %collective-permute-start.1) | collective-permute-done | bytes 1048608 | tf_op jit(solution)/shard_map/ppermute | solution.py:21
  261.8 21.6 %collective-permute-done.2 = bf16[256,2048]{1,0:T(8,128)(2,1)} collective-permute-done((bf16[256,2048]{1,0:T(8,128)(2,1)}, bf16[256,2048]{1,0:T(8,128)(2,1)}, u32[]{:S(2)}, u32[]{:S(2)}) %collective-permute-start.2) | collective-permute-done | bytes 1048608 | tf_op jit(solution)/shard_map/ppermute | solution.py:21
  283.4 2.3 constant_dynamic-update-slice_fusion.7
  285.8 2.3 constant_dynamic-update-slice_fusion.6
  288.1 1.0 constant_dynamic-update-slice_fusion.5
  289.1 1.2 constant_dynamic-update-slice_fusion.4
  290.4 2.3 constant_dynamic-update-slice_fusion.3
  292.7 2.3 constant_dynamic-update-slice_fusion.2
  295.0 1.0 constant_dynamic-update-slice_fusion.1
  296.0 1.3 constant_dynamic-update-slice_fusion
  297.3 11.7 %fusion.21 = f32[1024,1408]{1,0:T(8,128)} fusion(bf16[2048,4224]{1,0:T(8,128)(2,1)} %all-gather.11.cloned.1.call-done, bf16[2048,2048]{1,0:T(8,128)(2,1)} %constant_dynamic-update-slice_fusion, s32[]{:T(128)S(6)} %select_n.2247), kind=kOutput, calls=%fused_computation.48 | convolution fusion | flops 5905580032 | bytes 15728644 | tf_op jit(solution)/shard_map/dot_general | solution.py:238
  309.0 20.6 %fusion.23 = bf16[1024,2048]{1,0:T(8,128)(2,1)} fusion(bf16[2048,4224]{1,0:T(8,128)(2,1)} %all-gather.11.cloned.1.call-done, f32[1024,1408]{1,0:T(8,128)} %fusion.21, bf16[2048,2048]{1,0:T(8,128)(2,1)} %constant_dynamic-update-slice_fusion, s32[]{:T(128)S(6)} %select_n.2247), kind=kOutput, calls=%fused_computation.51 | convolution fusion | flops 11821907968 | bytes 25690116 | tf_op jit(solution)/shard_map/dot_general | solution.py:241
  329.7 54.6 %reduce-scatter.2.cloned.1.call-done = bf16[256,2048]{1,0:T(8,128)(2,1)} async-done(((bf16[1024,2048]{1,0:T(8,128)(2,1)}), bf16[256,2048]{1,0:T(8,128)(2,1)}) %reduce-scatter.2.cloned.1.call-update) | async-done | bytes 1048592 | tf_op jit(solution)/shard_map/reduce_scatter | solution.py:242
  384.3 2.5 add_convert_fusion
  (288 shorter events, 69.3 us)
Async XLA Ops:
  6.5 212.0 %all-gather.9.cloned.1.call-start = ((), (), s32[]{:S(2)}) async-start(), calls=%async_computation.2 | async-start | bytes 5242880 | tf_op jit(solution)/shard_map/all_gather | solution.py:231
  7.3 290.1 %all-gather.11.cloned.1.call-start = ((), (), s32[]{:S(2)}) async-start(), calls=%async_computation.3 | async-start | bytes 17842176 | tf_op jit(solution)/shard_map/all_gather | solution.py:30
  9.2 66.4 %copy-start = (bf16[1024,256]{1,0:T(8,128)(2,1)S(1)}, bf16[1024,256]{1,0:T(8,128)(2,1)}, u32[]{:S(2)}) copy-start(bf16[1024,256]{1,0:T(8,128)(2,1)} %param.16) | copy-start | bytes 1572868
  41.0 35.1 %copy-start.2 = (bf16[1024,256]{1,0:T(8,128)(2,1)S(1)}, bf16[1024,256]{1,0:T(8,128)(2,1)}, u32[]{:S(2)}) copy-start(bf16[1024,256]{1,0:T(8,128)(2,1)} %param.17) | copy-start | bytes 1572868
  43.7 34.0 %copy-start.6 = (f32[2,1024]{1,0:T(2,128)S(1)}, f32[2,1024]{1,0:T(2,128)}, u32[]{:S(2)}) copy-start(f32[2,1024]{1,0:T(2,128)} %param.19) | copy-start | bytes 24580
  43.7 34.0 %copy-start.8 = (u32[128]{0:T(128)S(1)}, u32[128]{0:T(128)}, u32[]{:S(2)}) copy-start(u32[128]{0:T(128)} %constant.134) | copy-start | bytes 1540
  72.4 0.8 copy-start.1
  76.1 24.0 %copy-start.3 = (f32[1,256,128]{2,1,0:T(8,128)S(1)}, f32[1,256,128]{2,1,0:T(8,128)}, u32[]{:S(2)}) copy-start(f32[1,256,128]{2,1,0:T(8,128)} %get-tuple-element.183) | copy-start | bytes 393220
  76.1 24.0 %copy-start.4 = (f32[1,256,128]{2,1,0:T(8,128)S(1)}, f32[1,256,128]{2,1,0:T(8,128)}, u32[]{:S(2)}) copy-start(f32[1,256,128]{2,1,0:T(8,128)} %get-tuple-element.184) | copy-start | bytes 393220
  76.1 24.0 %copy-start.5 = (f32[1,256,128]{2,1,0:T(8,128)S(1)}, f32[1,256,128]{2,1,0:T(8,128)}, u32[]{:S(2)}) copy-start(f32[1,256,128]{2,1,0:T(8,128)} %get-tuple-element.171) | copy-start | bytes 393220
  101.9 109.7 %copy-start.7 = (bf16[2048]{0:T(1024)(128)(2,1)S(1)}, bf16[2048]{0:T(1024)(128)(2,1)}, u32[]{:S(2)}) copy-start(bf16[2048]{0:T(1024)(128)(2,1)} %param.24) | copy-start | bytes 12292
  207.8 10.6 %all-to-all-start = ((bf16[4,256,256]{1,2,0:T(8,128)(2,1)}), bf16[4,256,256]{1,2,0:T(8,128)(2,1)S(1)}, u32[]{:S(2)}, u32[]{:S(2)}) async-start(bf16[4,256,256]{1,2,0:T(8,128)(2,1)} %bitcast.514), calls=%async_computation | async-start | bytes 1048576 | tf_op jit(solution)/shard_map/all_to_all | solution.py:228
  211.6 172.7 %reduce-scatter.2.cloned.1.call-start = ((), (), s32[]{:S(2)}) async-start(), calls=%async_computation.4 | async-start | bytes 5242880 | tf_op jit(solution)/shard_map/reduce_scatter | solution.py:242
  222.6 17.5 %collective-permute-start = (bf16[256,2048]{1,0:T(8,128)(2,1)S(1)}, bf16[256,2048]{1,0:T(8,128)(2,1)S(1)}, u32[]{:S(2)}, u32[]{:S(2)}) collective-permute-start(bf16[256,2048]{1,0:T(8,128)(2,1)S(1)} %multiply_convert_fusion.1), channel_id=1, source_target_pairs={{0,1},{1,2},{2,3},{3,0},{4,5},{5,6},{6,7},{7,4},{8,9},{9,10},{10,1... | collective-permute-start | bytes 3145736 | tf_op jit(solution)/shard_map/ppermute | solution.py:21
  240.1 21.7 %collective-permute-start.1 = (bf16[256,2048]{1,0:T(8,128)(2,1)S(1)}, bf16[256,2048]{1,0:T(8,128)(2,1)}, u32[]{:S(2)}, u32[]{:S(2)}) collective-permute-start(bf16[256,2048]{1,0:T(8,128)(2,1)S(1)} %collective-permute-done), channel_id=1, source_target_pairs={{0,1},{1,2},{2,3},{3,0},{4,5},{5,6},{6,7},{7,4},{8,9},{9,10},{10,1... | collective-permute-start | bytes 3145736 | tf_op jit(solution)/shard_map/ppermute | solution.py:21
  261.8 21.6 %collective-permute-start.2 = (bf16[256,2048]{1,0:T(8,128)(2,1)}, bf16[256,2048]{1,0:T(8,128)(2,1)}, u32[]{:S(2)}, u32[]{:S(2)}) collective-permute-start(bf16[256,2048]{1,0:T(8,128)(2,1)} %collective-permute-done.1), channel_id=1, source_target_pairs={{0,1},{1,2},{2,3},{3,0},{4,5},{5,6},{6,7},{7,4},{8,9},{9,10},{10,1... | collective-permute-start | bytes 3145736 | tf_op jit(solution)/shard_map/ppermute | solution.py:21
Sparse Core Ops, SparseCore 0:
  9.0 51.1 all-gather.8
  62.5 74.8 all-gather.10
  329.8 54.4 reduce-scatter.1
